TPU v7x, 32 devices: a whole 2x2x4 slice. The times are simulated.
32 devices in a mesh: sp: 8 (over z, y), tp: 4 (over x, core).
Axes of the slice: x: 2, y: 2, z: 4, core: 2. Of those that a mesh axis runs over, the one named last changes fastest.
Arguments:
- stream: bfloat16 [3072, 2048], P(('sp', 'tp')), may hold values from -6 to 6
- query_projected: bfloat16 [3072, 1024], P('sp', 'tp'), may hold values from -6 to 6
- key_projected: bfloat16 [3072, 1024], P('sp', 'tp'), may hold values from -6 to 6
- value_projected: bfloat16 [3072, 1024], P('sp', 'tp'), may hold values from -6 to 6
- gate_projected: bfloat16 [3072, 1024], P('sp', 'tp'), may hold values from -6 to 6
- strength_logits: bfloat16 [8, 3072], P('tp', 'sp'), may hold values from -7 to 4
- decay_preactivation: bfloat16 [8, 3072], P('tp', 'sp'), may hold values from -9 to 9
- extra_log_decay: float32 [8, 3072], P('tp', 'sp'), may hold values from -0.7 to 0
- head_decay_rate: float32 [8], P('tp'), may hold values from 0 to 0.1
- head_norm_gain: float32 [128], replicated, may hold values from 0.1 to 1.9
- head_output_matrix: bfloat16 [1024, 2048], P('tp'), may hold values from -0.1875 to 0.1875
- feed_norm_gain: float32 [2048], replicated, may hold values from 0.1 to 1.9
- gate_matrix: bfloat16 [2048, 5632], P('sp', 'tp'), may hold values from -0.125 to 0.125
- up_matrix: bfloat16 [2048, 5632], P('sp', 'tp'), may hold values from -0.125 to 0.125
- down_matrix: bfloat16 [5632, 2048], P('tp', 'sp'), may hold values from -0.078125 to 0.078125
Outputs:
- result: bfloat16 [3072, 2048], P(('sp', 'tp'))
All inputs are finite; a program needn't handle non-finite values.
Results may differ from a plain program's by a relative error of at most 0.015.
Values may be sent and summed in bfloat16 or wider, within the bound.
No kernel may reach another device: no remote copies, remote signals or barrier semaphores. Data moves between devices by JAX's collectives and lax.ppermute only.
A program may use at most 128 MiB of HBM per device.

v0:
```python
import jax
import jax.numpy as jnp
from jax import lax
from jax.sharding import PartitionSpec as P

HEAD = 128
BLOCK = 64
PRECISION_FULL = lax.Precision.HIGHEST
EPSILON = 1e-06


def from_behind(value, axis, by):
    size = lax.axis_size(axis)
    pairs = [(i, i + by) for i in range(size) if 0 <= i + by < size]
    return lax.ppermute(value, axis, pairs)


def unit_rows(tensor):
    return tensor * lax.rsqrt(jnp.sum(tensor * tensor, axis=-1, keepdims=True) + EPSILON)


def rms_scale(tensor):
    return tensor * lax.rsqrt(jnp.mean(tensor * tensor, axis=-1, keepdims=True) + EPSILON)


def block_correction(
    unit_queries,
    unit_keys,
    complete_values,
    strength_logits,
    decay_preactivation,
    extra_log_decay,
    head_decay_rate,
):
    head_count, length, head_width = unit_queries.shape
    block_count = length // BLOCK

    def to_blocks(tensor):
        return tensor.reshape((head_count, block_count, BLOCK) + tensor.shape[2:])

    beta_gate = jax.nn.sigmoid(strength_logits.astype(jnp.float32))
    decay_logarithm = (
        -head_decay_rate[:, None] * jax.nn.softplus(decay_preactivation.astype(jnp.float32))
        + extra_log_decay
    )
    query_block = to_blocks(unit_queries)
    key_block = to_blocks(unit_keys)
    value_block = to_blocks(complete_values)
    beta_block = to_blocks(beta_gate)
    cumulative = jnp.cumsum(to_blocks(decay_logarithm), axis=-1)
    causal = jnp.tril(jnp.ones((BLOCK, BLOCK), bool))
    strict = jnp.tril(jnp.ones((BLOCK, BLOCK), bool), -1)
    spread = cumulative[..., :, None] - cumulative[..., None, :]
    damping = jnp.where(causal, jnp.exp(jnp.where(causal, spread, 0.0)), 0.0)
    key_beta = key_block * beta_block[..., None]
    lower_part = jnp.einsum(
        "hnid,hnjd->hnij", key_beta, key_block, precision=PRECISION_FULL
    ) * jnp.where(strict, damping, 0.0)
    system = lower_part + jnp.eye(BLOCK, dtype=jnp.float32)
    right_side = jnp.concatenate(
        [value_block * beta_block[..., None], key_beta * jnp.exp(cumulative)[..., None]], axis=-1
    )
    solved = lax.linalg.triangular_solve(
        system, right_side, left_side=True, lower=True, unit_diagonal=True
    )
    target_values = solved[..., :head_width]
    householder_weights = solved[..., head_width:]
    inner_scores = (
        jnp.einsum("hnid,hnjd->hnij", query_block, key_block, precision=PRECISION_FULL) * damping
    )
    decayed_queries = query_block * jnp.exp(cumulative)[..., None]
    closing_log_decay = cumulative[..., -1:]
    decayed_keys = key_block * jnp.exp(closing_log_decay - cumulative)[..., None]
    return (
        decayed_queries,
        decayed_keys,
        target_values,
        householder_weights,
        inner_scores,
        closing_log_decay,
    )


def local_recurrence(
    query_projected,
    key_projected,
    value_projected,
    strength_logits,
    decay_preactivation,
    extra_log_decay,
    head_decay_rate,
):
    head_count = strength_logits.shape[0]
    tok_count = strength_logits.shape[1]

    def split_heads(tensor):
        return tensor.reshape(tok_count, head_count, HEAD).transpose(1, 0, 2).astype(jnp.float32)

    unit_queries = unit_rows(split_heads(query_projected)) * HEAD ** (-0.5)
    unit_keys = unit_rows(split_heads(key_projected))
    complete_values = split_heads(value_projected)
    score_terms = block_correction(
        unit_queries,
        unit_keys,
        complete_values,
        strength_logits,
        decay_preactivation,
        extra_log_decay,
        head_decay_rate,
    )
    identity = jnp.broadcast_to(jnp.eye(HEAD, dtype=jnp.float32), (head_count, HEAD, HEAD))

    def advance(carry, items):
        running_state, matrix_product = carry
        (
            decayed_queries,
            decayed_keys,
            target_values,
            householder_weights,
            inner_scores,
            closing_log_decay,
        ) = items
        new_state = target_values - jnp.einsum(
            "fdc,fcj->fdj", householder_weights, running_state, precision=PRECISION_FULL
        )
        layer_output = jnp.einsum(
            "fdc,fcj->fdj", decayed_queries, running_state, precision=PRECISION_FULL
        )
        layer_output = layer_output + jnp.einsum(
            "hij,hjv->hiv", inner_scores, new_state, precision=PRECISION_FULL
        )
        passed_state = decayed_queries - jnp.einsum(
            "hij,hjk->hik", inner_scores, householder_weights, precision=PRECISION_FULL
        )
        decay_span = jnp.einsum(
            "fdc,fcj->fdj", passed_state, matrix_product, precision=PRECISION_FULL
        )
        decay_factor = jnp.exp(closing_log_decay)[:, :, None]
        step_map = decay_factor * identity - jnp.einsum(
            "hik,hij->hkj", decayed_keys, householder_weights, precision=PRECISION_FULL
        )
        running_state = decay_factor * running_state + jnp.einsum(
            "xwp,xws->xps", decayed_keys, new_state, precision=PRECISION_FULL
        )
        matrix_product = jnp.einsum(
            "hij,hjk->hik", step_map, matrix_product, precision=PRECISION_FULL
        )
        return ((running_state, matrix_product), (layer_output, decay_span))

    moved = tuple((jnp.moveaxis(tensor, 1, 0) for tensor in score_terms))
    zeros_state = jnp.zeros((head_count, HEAD, HEAD), jnp.float32)
    (running_state, matrix_product), (block_outputs, decay_spans) = lax.scan(
        advance, (zeros_state, identity), moved
    )

    def merge_blocks(tensor):
        return jnp.moveaxis(tensor, 0, 1).reshape(head_count, tok_count, HEAD)

    return (
        merge_blocks(block_outputs),
        merge_blocks(decay_spans),
        matrix_product,
        running_state,
        identity,
    )


def feed_forward(whole_rows, gate_matrix, up_matrix, down_matrix):
    gate_whole, up_whole = (
        lax.all_gather(gate_matrix, "sp", axis=0, tiled=True),
        lax.all_gather(up_matrix, "sp", axis=0, tiled=True),
    )
    gate_total = jnp.dot(whole_rows, gate_whole, preferred_element_type=jnp.float32)
    up_total = jnp.dot(whole_rows, up_whole, preferred_element_type=jnp.float32)
    hidden = (jax.nn.silu(gate_total) * up_total).astype(jnp.bfloat16)
    down_whole = lax.all_gather(down_matrix, "sp", axis=1, tiled=True)
    return jnp.dot(hidden, down_whole, preferred_element_type=jnp.float32)


def body(
    stream,
    query_projected,
    key_projected,
    value_projected,
    gate_projected,
    strength_logits,
    decay_preactivation,
    extra_log_decay,
    head_decay_rate,
    head_norm_gain,
    head_output_matrix,
    feed_norm_gain,
    gate_matrix,
    up_matrix,
    down_matrix,
):
    block_outputs, decay_spans, matrix_product, running_state, identity = local_recurrence(
        query_projected,
        key_projected,
        value_projected,
        strength_logits,
        decay_preactivation,
        extra_log_decay,
        head_decay_rate,
    )
    zeros_state = jnp.zeros_like(running_state)

    def pass_state(turn, state_inflow):
        leaving = (
            jnp.einsum("hij,hjk->hik", matrix_product, state_inflow, precision=PRECISION_FULL)
            + running_state
        )
        return from_behind(leaving.astype(jnp.bfloat16), "sp", 1).astype(leaving.dtype)

    state_inflow = lax.fori_loop(0, lax.axis_size("sp") - 1, pass_state, zeros_state)
    attention_output = block_outputs + jnp.einsum(
        "qwc,qcn->qwn", decay_spans, state_inflow, precision=PRECISION_FULL
    )
    head_count = attention_output.shape[0]
    tok_count = attention_output.shape[1]
    normed_heads = rms_scale(attention_output) * head_norm_gain
    gated = normed_heads.transpose(1, 0, 2).reshape(tok_count, head_count * HEAD)
    mixed = (gated * jax.nn.silu(gate_projected.astype(jnp.float32))).astype(jnp.bfloat16)
    branch = lax.psum_scatter(
        jnp.dot(mixed, head_output_matrix, preferred_element_type=jnp.float32).astype(jnp.bfloat16),
        "tp",
        scatter_dimension=0,
        tiled=True,
    ).astype(jnp.float32)
    residual_own = stream.astype(jnp.float32) + branch
    normed_own = (rms_scale(residual_own) * feed_norm_gain).astype(jnp.bfloat16)
    whole_rows = lax.all_gather(normed_own, "tp", axis=0, tiled=True)
    ffn_term = feed_forward(whole_rows, gate_matrix, up_matrix, down_matrix)
    ffn_own = lax.psum_scatter(
        ffn_term.astype(jnp.bfloat16), "tp", scatter_dimension=0, tiled=True
    ).astype(jnp.float32)
    return (residual_own + ffn_own).astype(jnp.bfloat16)


def solution(mesh):
    placed = (
        P(("sp", "tp"), None),
        P("sp", "tp"),
        P("sp", "tp"),
        P("sp", "tp"),
        P("sp", "tp"),
        P("tp", "sp"),
        P("tp", "sp"),
        P("tp", "sp"),
        P("tp"),
        P(),
        P("tp", None),
        P(),
        P("sp", "tp"),
        P("sp", "tp"),
        P("tp", "sp"),
    )
    return jax.shard_map(
        body, mesh=mesh, in_specs=placed, out_specs=P(("sp", "tp"), None), check_vma=False
    )
```

profile of v0, /device:TPU:0, one launch (start us, length us, event | category | flops | bytes accessed | tf_op | source)
XLA Modules:
  0.0 551.2 jit_solution(7347479485389619198)
XLA Ops:
  8.9 1.1 fusion.64
  10.0 1.1 fusion.62
  11.1 1.1 fusion.60
  12.2 1.1 fusion.61
  14.1 1.0 copy_bitcast_fusion
  16.0 59.6 %custom-call.3 = f32[2,6,1,64,64]{3,4,2,1,0:T(8,128)} custom-call(f32[2,6,1,64,64]{4,3,2,1,0:T(8,128)S(1)} %fusion.48), custom_call_target="InvertDiagBlocksLowerTriangular" | custom-call | tf_op jit(solution)/shard_map/triangular_solve | solution.py:63
  75.6 1.1 multiply_multiply_fusion
  76.7 0.9 fusion.49
  77.6 0.8 slice_bitcast_fusion
  79.3 36.4 %while.28 = (s32[]{:T(128)}, f32[2,128,128]{2,1,0:T(8,128)S(1)}, f32[2,128,128]{2,1,0:T(8,128)S(1)}, f32[6,2,64,128]{3,2,0,1:T(8,128)}, f32[6,2,64,128]{3,2,0,1:...) while((s32[]{:T(128)}, f32[2,128,128]{2,1,0:T(8,128)S(1)}, ...), condition=%wide.region_4.5_spmd.clone, body=%wide.region_3.4_spmd.clone.sunk | while | flops 201605120 | bytes 2759337 | solution.py:152
  79.4 1.1 convolution_subtract_fusion.6
  80.5 1.1 fusion.145
  81.5 0.8 fusion.146
  82.8 1.0 convolution_subtract_fusion.8
  83.9 0.9 fusion.147
  85.4 1.1 convolution_subtract_fusion.6
  86.5 1.1 fusion.145
  87.6 0.8 fusion.146
  88.9 1.0 convolution_subtract_fusion.8
  89.9 0.9 fusion.147
  91.5 1.1 convolution_subtract_fusion.6
  92.6 1.1 fusion.145
  94.9 1.0 convolution_subtract_fusion.8
  96.0 0.9 fusion.147
  97.5 1.1 convolution_subtract_fusion.6
  98.6 1.1 fusion.145
  101.0 1.0 convolution_subtract_fusion.8
  102.0 0.9 fusion.147
  103.6 1.1 convolution_subtract_fusion.6
  104.7 1.1 fusion.145
  107.0 1.0 convolution_subtract_fusion.8
  108.1 0.9 fusion.147
  109.7 1.1 convolution_subtract_fusion.6
  110.7 1.1 fusion.145
  113.1 1.0 convolution_subtract_fusion.8
  114.2 0.9 fusion.147
  115.7 1.2 copy.42
  116.9 49.8 %while.29 = (s32[]{:T(128)}, f32[2,128,128]{2,1,0:T(8,128)S(1)}, f32[2,128,128]{2,1,0:T(8,128)S(1)}, f32[2,128,128]{2,1,0:T(8,128)S(1)}, s32[]{:T(128)}, /*index=5*/s32[]{:T(128)}) while((s32[]{:T(128)}, f32[2,128,128]{2,1,0:T(8,128)S(1)}, f32[2,128,128]{2,1,0:T(8,128)S(1)}, f32[2,128,128]{2,1,0:T(8,128)S(1)}, s32[]{:T(128)}, ...), condition=%wide.region_6.7_spmd.clone, body=%wide.region_5.6_spmd.clone.sunk | while | flops 50462720 | bytes 917623 | solution.py:215
  117.2 4.9 collective-permute-start
  122.1 1.9 collective-permute-done
  124.3 4.3 collective-permute-start
  128.6 1.9 collective-permute-done
  130.8 4.3 collective-permute-start
  135.1 1.9 collective-permute-done
  137.3 5.2 collective-permute-start
  142.5 1.9 collective-permute-done
  144.7 5.2 collective-permute-start
  149.9 1.9 collective-permute-done
  152.1 5.3 collective-permute-start
  157.3 2.1 collective-permute-done
  159.7 5.1 collective-permute-start
  164.8 1.9 collective-permute-done
  167.8 1.8 convolution_convert_fusion.1
  169.6 31.9 %reduce-scatter.3.cloned.1.call-done = bf16[96,2048]{1,0:T(8,128)(2,1)} async-done(((bf16[384,2048]{1,0:T(8,128)(2,1)}), bf16[96,2048]{1,0:T(8,128)(2,1)}) %reduce-scatter.3.cloned.1.call-update) | async-done | bytes 393232 | tf_op jit(solution)/shard_map/reduce_scatter | solution.py:224
  201.5 1.2 multiply_reduce_fusion
  202.8 1.9 multiply_convert_fusion
  206.8 17.7 %all-gather.5.cloned.1.call-done = bf16[384,2048]{1,0:T(8,128)(2,1)} async-done(((bf16[96,2048]{1,0:T(8,128)(2,1)}), bf16[384,2048]{1,0:T(8,128)(2,1)}) %all-gather.5.cloned.1.call-update) | async-done | bytes 1572880 | tf_op jit(solution)/shard_map/all_gather | solution.py:232
  224.5 94.5 %all-gather.7.cloned.1.call-done = bf16[2048,1408]{1,0:T(8,128)(2,1)} async-done(((bf16[256,1408]{1,0:T(8,128)(2,1)}), bf16[2048,1408]{1,0:T(8,128)(2,1)}) %all-gather.7.cloned.1.call-update) | async-done | bytes 5767184 | tf_op jit(solution)/shard_map/all_gather | solution.py:170
  319.0 7.1 %fusion.84 = f32[384,1408]{1,0:T(8,128)} fusion(bf16[384,2048]{1,0:T(8,128)(2,1)} %all-gather.5.cloned.1.call-done, bf16[2048,1408]{1,0:T(8,128)(2,1)} %all-gather.7.cloned.1.call-done), kind=kOutput, calls=%fused_computation.133 | convolution fusion | flops 2214592512 | bytes 9502720 | tf_op jit(solution)/shard_map/dot_general | solution.py:173
  326.1 86.2 %all-gather.11.cloned.1.call-done = bf16[1408,2048]{1,0:T(8,128)(2,1)} async-done(((bf16[1408,256]{1,0:T(8,128)(2,1)}), bf16[1408,2048]{1,0:T(8,128)(2,1)}) %all-gather.11.cloned.1.call-update) | async-done | bytes 5767184 | tf_op jit(solution)/shard_map/all_gather | solution.py:176
  412.3 92.6 %all-gather.9.cloned.1.call-done = bf16[2048,1408]{1,0:T(8,128)(2,1)} async-done(((bf16[256,1408]{1,0:T(8,128)(2,1)}), bf16[2048,1408]{1,0:T(8,128)(2,1)}) %all-gather.9.cloned.1.call-update) | async-done | bytes 5767184 | tf_op jit(solution)/shard_map/all_gather | solution.py:171
  504.8 11.3 %convolution_convert_fusion = bf16[384,2048]{1,0:T(8,128)(2,1)} fusion(bf16[1408,2048]{1,0:T(8,128)(2,1)} %all-gather.11.cloned.1.call-done, bf16[384,2048]{1,0:T(8,128)(2,1)S(1)} %copy-done.7, bf16[2048,1408]{1,0:T(8,128)(2,1)} %all-gather.9.cloned.1.call-done, f32[384,1408]{1,0:T(8,128)} %fusion.84), kind=kOutput, calls=%fused_computation.52 | convolution fusion | flops 4433215488 | bytes 16842752 | tf_op jit(solution)/shard_map/dot_general | solution.py:177
  516.1 26.4 %reduce-scatter.5.cloned.1.call-done = bf16[96,2048]{1,0:T(8,128)(2,1)} async-done(((bf16[384,2048]{1,0:T(8,128)(2,1)}), bf16[96,2048]{1,0:T(8,128)(2,1)}) %reduce-scatter.5.cloned.1.call-update) | async-done | bytes 393232 | tf_op jit(solution)/shard_map/reduce_scatter | solution.py:234
  542.5 1.9 add_convert_fusion
  (105 shorter events, 19.7 us)
Async XLA Ops:
  6.5 161.2 %copy-start = (bf16[256,2048]{1,0:T(8,128)(2,1)S(1)}, bf16[256,2048]{1,0:T(8,128)(2,1)}, u32[]{:S(2)}) copy-start(bf16[256,2048]{1,0:T(8,128)(2,1)} %param.29) | copy-start | bytes 3145732
  6.5 195.0 %reduce-scatter.3.cloned.1.call-start = ((), (), s32[]{:S(2)}) async-start(), calls=%async_computation.2 | async-start | bytes 1966080 | tf_op jit(solution)/shard_map/reduce_scatter | solution.py:224
  75.6 1.1 copy-start.4
  115.7 51.0 %copy-start.3 = (f32[6,2,64,128]{3,2,0,1:T(8,128)S(1)}, f32[6,2,64,128]{3,2,0,1:T(8,128)}, u32[]{:S(2)}) copy-start(f32[6,2,64,128]{3,2,0,1:T(8,128)} %get-tuple-element.93) | copy-start | bytes 1179652
  116.9 50.5 %copy-start.6 = (f32[128]{0:T(128)S(1)}, f32[128]{0:T(128)}, u32[]{:S(2)}) copy-start(f32[128]{0:T(128)} %param.28) | copy-start | bytes 1540
  117.2 6.8 %collective-permute-start = (bf16[2,128,128]{2,1,0:T(8,128)(2,1)S(1)}, bf16[2,128,128]{2,1,0:T(8,128)(2,1)S(1)}, u32[]{:S(2)}, u32[]{:S(2)}) collective-permute-start(bf16[2,128,128]{2,1,0:T(8,128)(2,1)S(1)} %fusion.150), channel_id=1, source_target_pairs={{0,4},{4,8},{8,12},{12,16},{16,20},{20,24},{24,28},{1,5},{5,9},{9,... | collective-permute-start | bytes 196616 | tf_op jit(solution)/shard_map/while/body/eval_jaxpr/ppermute | solution.py:15
  124.3 6.2 %collective-permute-start = (bf16[2,128,128]{2,1,0:T(8,128)(2,1)S(1)}, bf16[2,128,128]{2,1,0:T(8,128)(2,1)S(1)}, u32[]{:S(2)}, u32[]{:S(2)}) collective-permute-start(bf16[2,128,128]{2,1,0:T(8,128)(2,1)S(1)} %fusion.150), channel_id=1, source_target_pairs={{0,4},{4,8},{8,12},{12,16},{16,20},{20,24},{24,28},{1,5},{5,9},{9,... | collective-permute-start | bytes 196616 | tf_op jit(solution)/shard_map/while/body/eval_jaxpr/ppermute | solution.py:15
  130.8 6.2 %collective-permute-start = (bf16[2,128,128]{2,1,0:T(8,128)(2,1)S(1)}, bf16[2,128,128]{2,1,0:T(8,128)(2,1)S(1)}, u32[]{:S(2)}, u32[]{:S(2)}) collective-permute-start(bf16[2,128,128]{2,1,0:T(8,128)(2,1)S(1)} %fusion.150), channel_id=1, source_target_pairs={{0,4},{4,8},{8,12},{12,16},{16,20},{20,24},{24,28},{1,5},{5,9},{9,... | collective-permute-start | bytes 196616 | tf_op jit(solution)/shard_map/while/body/eval_jaxpr/ppermute | solution.py:15
  137.3 7.1 %collective-permute-start = (bf16[2,128,128]{2,1,0:T(8,128)(2,1)S(1)}, bf16[2,128,128]{2,1,0:T(8,128)(2,1)S(1)}, u32[]{:S(2)}, u32[]{:S(2)}) collective-permute-start(bf16[2,128,128]{2,1,0:T(8,128)(2,1)S(1)} %fusion.150), channel_id=1, source_target_pairs={{0,4},{4,8},{8,12},{12,16},{16,20},{20,24},{24,28},{1,5},{5,9},{9,... | collective-permute-start | bytes 196616 | tf_op jit(solution)/shard_map/while/body/eval_jaxpr/ppermute | solution.py:15
  144.7 7.1 %collective-permute-start = (bf16[2,128,128]{2,1,0:T(8,128)(2,1)S(1)}, bf16[2,128,128]{2,1,0:T(8,128)(2,1)S(1)}, u32[]{:S(2)}, u32[]{:S(2)}) collective-permute-start(bf16[2,128,128]{2,1,0:T(8,128)(2,1)S(1)} %fusion.150), channel_id=1, source_target_pairs={{0,4},{4,8},{8,12},{12,16},{16,20},{20,24},{24,28},{1,5},{5,9},{9,... | collective-permute-start | bytes 196616 | tf_op jit(solution)/shard_map/while/body/eval_jaxpr/ppermute | solution.py:15
  152.1 7.4 %collective-permute-start = (bf16[2,128,128]{2,1,0:T(8,128)(2,1)S(1)}, bf16[2,128,128]{2,1,0:T(8,128)(2,1)S(1)}, u32[]{:S(2)}, u32[]{:S(2)}) collective-permute-start(bf16[2,128,128]{2,1,0:T(8,128)(2,1)S(1)} %fusion.150), channel_id=1, source_target_pairs={{0,4},{4,8},{8,12},{12,16},{16,20},{20,24},{24,28},{1,5},{5,9},{9,... | collective-permute-start | bytes 196616 | tf_op jit(solution)/shard_map/while/body/eval_jaxpr/ppermute | solution.py:15
  159.7 7.0 %collective-permute-start = (bf16[2,128,128]{2,1,0:T(8,128)(2,1)S(1)}, bf16[2,128,128]{2,1,0:T(8,128)(2,1)S(1)}, u32[]{:S(2)}, u32[]{:S(2)}) collective-permute-start(bf16[2,128,128]{2,1,0:T(8,128)(2,1)S(1)} %fusion.150), channel_id=1, source_target_pairs={{0,4},{4,8},{8,12},{12,16},{16,20},{20,24},{24,28},{1,5},{5,9},{9,... | collective-permute-start | bytes 196616 | tf_op jit(solution)/shard_map/while/body/eval_jaxpr/ppermute | solution.py:15
  166.7 1.0 copy-start.8
  167.7 33.8 %copy-start.1 = (bf16[96,2048]{1,0:T(8,128)(2,1)S(1)}, bf16[96,2048]{1,0:T(8,128)(2,1)}, u32[]{:S(2)}) copy-start(bf16[96,2048]{1,0:T(8,128)(2,1)} %param.19) | copy-start | bytes 1179652
  167.7 35.0 %copy-start.5 = (f32[2048]{0:T(1024)S(1)}, f32[2048]{0:T(1024)}, u32[]{:S(2)}) copy-start(f32[2048]{0:T(1024)} %param.30) | copy-start | bytes 24580
  169.6 54.9 %all-gather.5.cloned.1.call-start = ((), (), s32[]{:S(2)}) async-start(), calls=%async_computation.3 | async-start | bytes 1966080 | tf_op jit(solution)/shard_map/all_gather | solution.py:232
  204.7 114.3 %all-gather.7.cloned.1.call-start = ((), (), s32[]{:S(2)}) async-start(), calls=%async_computation.4 | async-start | bytes 6488064 | tf_op jit(solution)/shard_map/all_gather | solution.py:170
  205.4 206.8 %all-gather.11.cloned.1.call-start = ((), (), s32[]{:S(2)}) async-start(), calls=%async_computation.6 | async-start | bytes 6488064 | tf_op jit(solution)/shard_map/all_gather | solution.py:176
  206.0 298.8 %all-gather.9.cloned.1.call-start = ((), (), s32[]{:S(2)}) async-start(), calls=%async_computation.5 | async-start | bytes 6488064 | tf_op jit(solution)/shard_map/all_gather | solution.py:171
  206.6 335.9 %reduce-scatter.5.cloned.1.call-start = ((), (), s32[]{:S(2)}) async-start(), calls=%async_computation.7 | async-start | bytes 1966080 | tf_op jit(solution)/shard_map/reduce_scatter | solution.py:234
  224.5 280.3 %copy-start.7 = (bf16[384,2048]{1,0:T(8,128)(2,1)S(1)}, bf16[384,2048]{1,0:T(8,128)(2,1)}, u32[]{:S(2)}) copy-start(bf16[384,2048]{1,0:T(8,128)(2,1)} %all-gather.5.cloned.1.call-done) | copy-start | bytes 4718596
  326.1 216.4 %copy-start.2 = (bf16[96,2048]{1,0:T(8,128)(2,1)S(1)}, bf16[96,2048]{1,0:T(8,128)(2,1)}, u32[]{:S(2)}) copy-start(bf16[96,2048]{1,0:T(8,128)(2,1)} %reduce-scatter.3.cloned.1.call-done) | copy-start | bytes 1179652
Sparse Core Ops, SparseCore 0:
  169.7 31.7 reduce-scatter.2
  204.8 19.6 all-gather.4
  226.7 92.3 all-gather.6
  320.9 91.2 all-gather.10
  414.3 90.4 all-gather.8
  516.2 26.1 reduce-scatter.4
where the time goes:
time: 553 us; the launch traced here: 551 us
  waiting for transfers between devices  364 us (66%)
  other arithmetic  74.1 us (13%)
  matrix products  60.9 us (11%)
  starting transfers between devices  34.5 us (6%)
  between operations  13.7 us (2%)
    all_gather x1, waiting for transfers between devices, feed_forward(): lax.all_gather(gate_matrix, 'sp', axis=0, tiled=True)  94.5 us
    all_gather x1, waiting for transfers between devices, feed_forward(): lax.all_gather(up_matrix, 'sp', axis=0, tiled=True)  92.6 us
    all_gather x1, waiting for transfers between devices, feed_forward(): down_whole = lax.all_gather(down_matrix, 'sp', axis=1, tiled=True)  86.2 us
    another operation x2, other arithmetic, block_correction(): lax.linalg.triangular_solve(system, right_side, left_side=True, lower=Tru...  59.6 us
    ppermute x7, starting transfers between devices, from_behind(): return lax.ppermute(value, axis, pairs)  34.2 us
    reduce_scatter x1, waiting for transfers between devices, body(): lax.psum_scatter(jnp.dot(mixed, head_output_matrix, preferred_element_typ...  31.9 us
    reduce_scatter x1, waiting for transfers between devices, body(): lax.psum_scatter(ffn_term.astype(jnp.bfloat16), 'tp', scatter_dimension=0...  26.4 us
    all_gather x1, waiting for transfers between devices, body(): whole_rows = lax.all_gather(normed_own, 'tp', axis=0, tiled=True)  17.7 us
  transfers between devices with their start and end apart: 13, of which 13 were waited for; matrix products, arithmetic and copies ran while one was open for 1% of the time, Pallas kernels for 0%

commit v1 on v0

--- a/solution.py
+++ b/solution.py
@@ -173,7 +173,7 @@
     gate_total = jnp.dot(whole_rows, gate_whole, preferred_element_type=jnp.float32)
     up_total = jnp.dot(whole_rows, up_whole, preferred_element_type=jnp.float32)
     hidden = (jax.nn.silu(gate_total) * up_total).astype(jnp.bfloat16)
-    down_whole = lax.all_gather(down_matrix, "sp", axis=1, tiled=True)
+    down_whole = jnp.concatenate(lax.all_gather(down_matrix, "sp"), 1)
     return jnp.dot(hidden, down_whole, preferred_element_type=jnp.float32)
 
 

time: 553 us -> 524 us (0.948)
  waiting for transfers between devices: 364 us -> 325 us
  local copies, waits for them, and re-layouts: 2.78 us -> 11.1 us
    all_gather x1, waiting for transfers between devices: 86.2 us -> 61.9 us  [feed_forward(): down_whole = jnp.concatenate(lax.all_gather(down_matrix, 'sp'), 1)]
    reshape x0 -> x1, local copies, waits for them, and re-layouts: none -> 8.34 us  [feed_forward(): down_whole = jnp.concatenate(lax.all_gather(down_matrix, 'sp'), 1)]
    all_gather x1, waiting for transfers between devices: 92.6 us -> 85.3 us  [feed_forward(): lax.all_gather(up_matrix, 'sp', axis=0, tiled=True)]
    all_gather x1, waiting for transfers between devices: 17.7 us -> 10.7 us  [body(): whole_rows = lax.all_gather(normed_own, 'tp', axis=0, tiled=True)]
  transfers between devices with their start and end apart: 13 -> 13, of which waited for: 13 -> 13; matrix products, arithmetic and copies ran while one was open for 1% -> 4% of each run, Pallas kernels for 0% -> 0%
where the time goes in v1:
time: 524 us; the launch traced here: 522 us
  waiting for transfers between devices  325 us (62%)
  other arithmetic  74.2 us (14%)
  matrix products  61 us (12%)
  starting transfers between devices  34.5 us (7%)
  between operations  15.3 us (3%)
  local copies, waits for them, and re-layouts  11.1 us (2%)
    all_gather x1, waiting for transfers between devices, feed_forward(): lax.all_gather(gate_matrix, 'sp', axis=0, tiled=True)  94.2 us
    all_gather x1, waiting for transfers between devices, feed_forward(): lax.all_gather(up_matrix, 'sp', axis=0, tiled=True)  85.3 us
    all_gather x1, waiting for transfers between devices, feed_forward(): down_whole = jnp.concatenate(lax.all_gather(down_matrix, 'sp'), 1)  61.9 us
    another operation x2, other arithmetic, block_correction(): lax.linalg.triangular_solve(system, right_side, left_side=True, lower=Tru...  59.6 us
    ppermute x7, starting transfers between devices, from_behind(): return lax.ppermute(value, axis, pairs)  34.2 us
    reduce_scatter x1, waiting for transfers between devices, body(): lax.psum_scatter(jnp.dot(mixed, head_output_matrix, preferred_element_typ...  31.3 us
    reduce_scatter x1, waiting for transfers between devices, body(): lax.psum_scatter(ffn_term.astype(jnp.bfloat16), 'tp', scatter_dimension=0...  26.4 us
    ppermute x7, waiting for transfers between devices, from_behind(): return lax.ppermute(value, axis, pairs)  13.4 us
  transfers between devices with their start and end apart: 13, of which 13 were waited for; matrix products, arithmetic and copies ran while one was open for 4% of the time, Pallas kernels for 0%

profile of v1, /device:TPU:0, one launch (start us, length us, event | category | flops | bytes accessed | tf_op | source)
XLA Modules:
  0.0 521.9 jit_solution(3108760313086860133)
XLA Ops:
  9.7 1.1 fusion.64
  10.8 1.1 fusion.62
  11.9 1.1 fusion.60
  13.1 1.1 fusion.61
  14.9 1.0 copy_bitcast_fusion
  16.8 59.6 %custom-call.3 = f32[2,6,1,64,64]{3,4,2,1,0:T(8,128)} custom-call(f32[2,6,1,64,64]{4,3,2,1,0:T(8,128)S(1)} %fusion.48), custom_call_target="InvertDiagBlocksLowerTriangular" | custom-call | tf_op jit(solution)/shard_map/triangular_solve | solution.py:63
  76.4 1.1 multiply_multiply_fusion
  77.6 0.9 fusion.49
  78.4 0.8 slice_bitcast_fusion
  80.2 36.4 %while.28 = (s32[]{:T(128)}, f32[2,128,128]{2,1,0:T(8,128)S(1)}, f32[2,128,128]{2,1,0:T(8,128)S(1)}, f32[6,2,64,128]{3,2,0,1:T(8,128)}, f32[6,2,64,128]{3,2,0,1:...) while((s32[]{:T(128)}, f32[2,128,128]{2,1,0:T(8,128)S(1)}, ...), condition=%wide.region_4.5_spmd.clone, body=%wide.region_3.4_spmd.clone.sunk | while | flops 201605120 | bytes 2759337 | solution.py:152
  80.2 1.1 convolution_subtract_fusion.6
  81.3 1.1 fusion.145
  82.4 0.8 fusion.146
  83.6 1.0 convolution_subtract_fusion.8
  84.7 0.9 fusion.147
  86.3 1.1 convolution_subtract_fusion.6
  87.3 1.1 fusion.145
  89.7 1.0 convolution_subtract_fusion.8
  90.8 0.9 fusion.147
  92.3 1.1 convolution_subtract_fusion.6
  93.4 1.1 fusion.145
  95.7 1.0 convolution_subtract_fusion.8
  96.8 0.9 fusion.147
  98.4 1.1 convolution_subtract_fusion.6
  99.5 1.1 fusion.145
  101.8 1.0 convolution_subtract_fusion.8
  102.9 0.9 fusion.147
  104.4 1.1 convolution_subtract_fusion.6
  105.5 1.1 fusion.145
  107.9 1.0 convolution_subtract_fusion.8
  108.9 0.9 fusion.147
  110.5 1.1 convolution_subtract_fusion.6
  111.6 1.1 fusion.145
  113.9 1.0 convolution_subtract_fusion.8
  115.0 0.9 fusion.147
  116.5 1.2 copy.57
  117.8 49.8 %while.29 = (s32[]{:T(128)}, f32[2,128,128]{2,1,0:T(8,128)S(1)}, f32[2,128,128]{2,1,0:T(8,128)S(1)}, f32[2,128,128]{2,1,0:T(8,128)S(1)}, s32[]{:T(128)}, /*index=5*/s32[]{:T(128)}) while((s32[]{:T(128)}, f32[2,128,128]{2,1,0:T(8,128)S(1)}, f32[2,128,128]{2,1,0:T(8,128)S(1)}, f32[2,128,128]{2,1,0:T(8,128)S(1)}, s32[]{:T(128)}, ...), condition=%wide.region_6.7_spmd.clone, body=%wide.region_5.6_spmd.clone.sunk | while | flops 50462720 | bytes 917623 | solution.py:215
  118.1 4.9 collective-permute-start
  123.0 1.9 collective-permute-done
  125.2 4.3 collective-permute-start
  129.4 1.9 collective-permute-done
  131.6 4.3 collective-permute-start
  136.0 1.9 collective-permute-done
  138.2 5.2 collective-permute-start
  143.3 1.9 collective-permute-done
  145.5 5.2 collective-permute-start
  150.7 1.9 collective-permute-done
  152.9 5.3 %collective-permute-start = (bf16[2,128,128]{2,1,0:T(8,128)(2,1)S(1)}, bf16[2,128,128]{2,1,0:T(8,128)(2,1)S(1)}, u32[]{:S(2)}, u32[]{:S(2)}) collective-permute-start(bf16[2,128,128]{2,1,0:T(8,128)(2,1)S(1)} %fusion.150), channel_id=1, source_target_pairs={{0,4},{4,8},{8,12},{12,16},{16,20},{20,24},{24,28},{1,5},{5,9},{9,... | collective-permute-start | bytes 196616 | tf_op jit(solution)/shard_map/while/body/eval_jaxpr/ppermute | solution.py:15
  158.2 2.1 collective-permute-done
  160.6 5.1 collective-permute-start
  165.7 1.9 collective-permute-done
  168.6 1.8 convolution_convert_fusion.1
  171.0 31.3 %reduce-scatter.3.cloned.1.call-done = bf16[96,2048]{1,0:T(8,128)(2,1)} async-done(((bf16[384,2048]{1,0:T(8,128)(2,1)}), bf16[96,2048]{1,0:T(8,128)(2,1)}) %reduce-scatter.3.cloned.1.call-update) | async-done | bytes 393232 | tf_op jit(solution)/shard_map/reduce_scatter | solution.py:224
  202.4 1.2 multiply_reduce_fusion
  203.6 1.9 multiply_convert_fusion
  207.1 61.9 %all-gather.12.cloned.1.call-done = bf16[11264,256]{1,0:T(8,128)(2,1)} async-done(((bf16[1408,256]{1,0:T(8,128)(2,1)}), bf16[11264,256]{1,0:T(8,128)(2,1)}) %all-gather.12.cloned.1.call-update) | async-done | bytes 5767184 | tf_op jit(solution)/shard_map/all_gather | solution.py:176
  269.0 8.3 %copy.59 = bf16[1408,8,256]{0,2,1:T(8,128)(2,1)} copy(bf16[1408,8,256]{2,0,1:T(8,128)(2,1)} %bitcast.192) | data formatting | bytes 11534336 | tf_op jit(solution)/shard_map/reshape | solution.py:176
  277.4 10.7 %all-gather.6.cloned.1.call-done = bf16[384,2048]{1,0:T(8,128)(2,1)} async-done(((bf16[96,2048]{1,0:T(8,128)(2,1)}), bf16[384,2048]{1,0:T(8,128)(2,1)}) %all-gather.6.cloned.1.call-update) | async-done | bytes 1572880 | tf_op jit(solution)/shard_map/all_gather | solution.py:232
  288.1 94.2 %all-gather.8.cloned.1.call-done = bf16[2048,1408]{1,0:T(8,128)(2,1)} async-done(((bf16[256,1408]{1,0:T(8,128)(2,1)}), bf16[2048,1408]{1,0:T(8,128)(2,1)}) %all-gather.8.cloned.1.call-update) | async-done | bytes 5767184 | tf_op jit(solution)/shard_map/all_gather | solution.py:170
  382.3 7.2 %fusion.84 = f32[384,1408]{1,0:T(8,128)} fusion(bf16[384,2048]{1,0:T(8,128)(2,1)} %all-gather.6.cloned.1.call-done, bf16[2048,1408]{1,0:T(8,128)(2,1)} %all-gather.8.cloned.1.call-done), kind=kOutput, calls=%fused_computation.133 | convolution fusion | flops 2214592512 | bytes 9502720 | tf_op jit(solution)/shard_map/dot_general | solution.py:173
  389.5 85.3 %all-gather.10.cloned.1.call-done = bf16[2048,1408]{1,0:T(8,128)(2,1)} async-done(((bf16[256,1408]{1,0:T(8,128)(2,1)}), bf16[2048,1408]{1,0:T(8,128)(2,1)}) %all-gather.10.cloned.1.call-update) | async-done | bytes 5767184 | tf_op jit(solution)/shard_map/all_gather | solution.py:171
  474.9 11.2 %convolution_convert_fusion = bf16[384,2048]{1,0:T(8,128)(2,1)} fusion(bf16[1408,2048]{0,1:T(8,128)(2,1)} %bitcast.193, bf16[384,2048]{1,0:T(8,128)(2,1)S(1)} %copy-done.7, bf16[2048,1408]{1,0:T(8,128)(2,1)} %all-gather.10.cloned.1.call-done, f32[384,1408]{1,0:T(8,128)} %fusion.84), kind=kOutput, calls=%fused_computation.52 | convolution fusion | flops 4433215488 | bytes 16842752 | tf_op jit(solution)/shard_map/dot_general | solution.py:177
  486.1 26.4 %reduce-scatter.5.cloned.1.call-done = bf16[96,2048]{1,0:T(8,128)(2,1)} async-done(((bf16[384,2048]{1,0:T(8,128)(2,1)}), bf16[96,2048]{1,0:T(8,128)(2,1)}) %reduce-scatter.5.cloned.1.call-update) | async-done | bytes 393232 | tf_op jit(solution)/shard_map/reduce_scatter | solution.py:234
  512.4 1.9 add_convert_fusion
  (106 shorter events, 20.5 us)
Async XLA Ops:
  7.4 161.2 %copy-start = (bf16[256,2048]{1,0:T(8,128)(2,1)S(1)}, bf16[256,2048]{1,0:T(8,128)(2,1)}, u32[]{:S(2)}) copy-start(bf16[256,2048]{1,0:T(8,128)(2,1)} %param.29) | copy-start | bytes 3145732
  7.4 195.0 %reduce-scatter.3.cloned.1.call-start = ((), (), s32[]{:S(2)}) async-start(), calls=%async_computation.2 | async-start | bytes 1966080 | tf_op jit(solution)/shard_map/reduce_scatter | solution.py:224
  76.4 1.1 copy-start.4
  116.5 51.0 %copy-start.3 = (f32[6,2,64,128]{3,2,0,1:T(8,128)S(1)}, f32[6,2,64,128]{3,2,0,1:T(8,128)}, u32[]{:S(2)}) copy-start(f32[6,2,64,128]{3,2,0,1:T(8,128)} %get-tuple-element.93) | copy-start | bytes 1179652
  117.8 50.5 %copy-start.6 = (f32[128]{0:T(128)S(1)}, f32[128]{0:T(128)}, u32[]{:S(2)}) copy-start(f32[128]{0:T(128)} %param.28) | copy-start | bytes 1540
  118.1 6.8 %collective-permute-start = (bf16[2,128,128]{2,1,0:T(8,128)(2,1)S(1)}, bf16[2,128,128]{2,1,0:T(8,128)(2,1)S(1)}, u32[]{:S(2)}, u32[]{:S(2)}) collective-permute-start(bf16[2,128,128]{2,1,0:T(8,128)(2,1)S(1)} %fusion.150), channel_id=1, source_target_pairs={{0,4},{4,8},{8,12},{12,16},{16,20},{20,24},{24,28},{1,5},{5,9},{9,... | collective-permute-start | bytes 196616 | tf_op jit(solution)/shard_map/while/body/eval_jaxpr/ppermute | solution.py:15
  125.2 6.2 %collective-permute-start = (bf16[2,128,128]{2,1,0:T(8,128)(2,1)S(1)}, bf16[2,128,128]{2,1,0:T(8,128)(2,1)S(1)}, u32[]{:S(2)}, u32[]{:S(2)}) collective-permute-start(bf16[2,128,128]{2,1,0:T(8,128)(2,1)S(1)} %fusion.150), channel_id=1, source_target_pairs={{0,4},{4,8},{8,12},{12,16},{16,20},{20,24},{24,28},{1,5},{5,9},{9,... | collective-permute-start | bytes 196616 | tf_op jit(solution)/shard_map/while/body/eval_jaxpr/ppermute | solution.py:15
  131.6 6.2 %collective-permute-start = (bf16[2,128,128]{2,1,0:T(8,128)(2,1)S(1)}, bf16[2,128,128]{2,1,0:T(8,128)(2,1)S(1)}, u32[]{:S(2)}, u32[]{:S(2)}) collective-permute-start(bf16[2,128,128]{2,1,0:T(8,128)(2,1)S(1)} %fusion.150), channel_id=1, source_target_pairs={{0,4},{4,8},{8,12},{12,16},{16,20},{20,24},{24,28},{1,5},{5,9},{9,... | collective-permute-start | bytes 196616 | tf_op jit(solution)/shard_map/while/body/eval_jaxpr/ppermute | solution.py:15
  138.2 7.1 %collective-permute-start = (bf16[2,128,128]{2,1,0:T(8,128)(2,1)S(1)}, bf16[2,128,128]{2,1,0:T(8,128)(2,1)S(1)}, u32[]{:S(2)}, u32[]{:S(2)}) collective-permute-start(bf16[2,128,128]{2,1,0:T(8,128)(2,1)S(1)} %fusion.150), channel_id=1, source_target_pairs={{0,4},{4,8},{8,12},{12,16},{16,20},{20,24},{24,28},{1,5},{5,9},{9,... | collective-permute-start | bytes 196616 | tf_op jit(solution)/shard_map/while/body/eval_jaxpr/ppermute | solution.py:15
  145.5 7.1 %collective-permute-start = (bf16[2,128,128]{2,1,0:T(8,128)(2,1)S(1)}, bf16[2,128,128]{2,1,0:T(8,128)(2,1)S(1)}, u32[]{:S(2)}, u32[]{:S(2)}) collective-permute-start(bf16[2,128,128]{2,1,0:T(8,128)(2,1)S(1)} %fusion.150), channel_id=1, source_target_pairs={{0,4},{4,8},{8,12},{12,16},{16,20},{20,24},{24,28},{1,5},{5,9},{9,... | collective-permute-start | bytes 196616 | tf_op jit(solution)/shard_map/while/body/eval_jaxpr/ppermute | solution.py:15
  152.9 7.4 %collective-permute-start = (bf16[2,128,128]{2,1,0:T(8,128)(2,1)S(1)}, bf16[2,128,128]{2,1,0:T(8,128)(2,1)S(1)}, u32[]{:S(2)}, u32[]{:S(2)}) collective-permute-start(bf16[2,128,128]{2,1,0:T(8,128)(2,1)S(1)} %fusion.150), channel_id=1, source_target_pairs={{0,4},{4,8},{8,12},{12,16},{16,20},{20,24},{24,28},{1,5},{5,9},{9,... | collective-permute-start | bytes 196616 | tf_op jit(solution)/shard_map/while/body/eval_jaxpr/ppermute | solution.py:15
  160.6 7.0 %collective-permute-start = (bf16[2,128,128]{2,1,0:T(8,128)(2,1)S(1)}, bf16[2,128,128]{2,1,0:T(8,128)(2,1)S(1)}, u32[]{:S(2)}, u32[]{:S(2)}) collective-permute-start(bf16[2,128,128]{2,1,0:T(8,128)(2,1)S(1)} %fusion.150), channel_id=1, source_target_pairs={{0,4},{4,8},{8,12},{12,16},{16,20},{20,24},{24,28},{1,5},{5,9},{9,... | collective-permute-start | bytes 196616 | tf_op jit(solution)/shard_map/while/body/eval_jaxpr/ppermute | solution.py:15
  167.6 1.0 copy-start.8
  168.6 33.8 %copy-start.1 = (bf16[96,2048]{1,0:T(8,128)(2,1)S(1)}, bf16[96,2048]{1,0:T(8,128)(2,1)}, u32[]{:S(2)}) copy-start(bf16[96,2048]{1,0:T(8,128)(2,1)} %param.19) | copy-start | bytes 1179652
  170.4 33.2 %copy-start.5 = (f32[2048]{0:T(1024)S(1)}, f32[2048]{0:T(1024)}, u32[]{:S(2)}) copy-start(f32[2048]{0:T(1024)} %param.30) | copy-start | bytes 24580
  170.4 98.6 %all-gather.12.cloned.1.call-start = ((), (), s32[]{:S(2)}) async-start(), calls=%async_computation.7 | async-start | bytes 6488064 | tf_op jit(solution)/shard_map/all_gather | solution.py:176
  171.0 117.1 %all-gather.6.cloned.1.call-start = ((), (), s32[]{:S(2)}) async-start(), calls=%async_computation.3 | async-start | bytes 1966080 | tf_op jit(solution)/shard_map/all_gather | solution.py:232
  205.5 176.8 %all-gather.8.cloned.1.call-start = ((), (), s32[]{:S(2)}) async-start(), calls=%async_computation.4 | async-start | bytes 6488064 | tf_op jit(solution)/shard_map/all_gather | solution.py:170
  206.1 268.7 %all-gather.10.cloned.1.call-start = ((), (), s32[]{:S(2)}) async-start(), calls=%async_computation.5 | async-start | bytes 6488064 | tf_op jit(solution)/shard_map/all_gather | solution.py:171
  206.9 305.6 %reduce-scatter.5.cloned.1.call-start = ((), (), s32[]{:S(2)}) async-start(), calls=%async_computation.6 | async-start | bytes 1966080 | tf_op jit(solution)/shard_map/reduce_scatter | solution.py:234
  288.1 186.7 %copy-start.7 = (bf16[384,2048]{1,0:T(8,128)(2,1)S(1)}, bf16[384,2048]{1,0:T(8,128)(2,1)}, u32[]{:S(2)}) copy-start(bf16[384,2048]{1,0:T(8,128)(2,1)} %all-gather.6.cloned.1.call-done) | copy-start | bytes 4718596
  474.9 37.6 %copy-start.2 = (bf16[96,2048]{1,0:T(8,128)(2,1)S(1)}, bf16[96,2048]{1,0:T(8,128)(2,1)}, u32[]{:S(2)}) copy-start(bf16[96,2048]{1,0:T(8,128)(2,1)} %reduce-scatter.3.cloned.1.call-done) | copy-start | bytes 1179652
Sparse Core Ops, SparseCore 0:
  170.5 31.7 reduce-scatter.2
  486.2 26.1 reduce-scatter.4
Sparse Core Ops, SparseCore 1:
  173.1 95.9 all-gather.11
  270.5 17.6 all-gather.5
  290.2 92.1 all-gather.7
  384.6 90.2 all-gather.9
